TPU v7x, 512 devices: a whole 4x4x16 slice. The times are simulated.
512 devices in a mesh: fs: 64 (over z, y), tp: 8 (over x, core).
Axes of the slice: x: 4, y: 4, z: 16, core: 2. Of those that a mesh axis runs over, the one named last changes fastest.
Arguments:
- fwd_input: bfloat16 [8192, 2048], P('fs'), may hold values from -6 to 6
- saved_input: bfloat16 [8192, 2048], P('fs'), may hold values from -16 to 16
- out_cotangent: bfloat16 [8192, 2048], P('fs'), may hold values from -16 to 16
- up_weight: bfloat16 [2048, 4096], P('fs', 'tp'), may hold values from -0.125 to 0.125
- down_weight: bfloat16 [4096, 2048], P('tp', 'fs'), may hold values from -0.09375 to 0.09375
- up_grad_sum: float32 [2048, 4096], P('fs', 'tp'), may hold values from -6 to 6
Outputs:
- layer_out: bfloat16 [8192, 2048], P('fs')
- input_grad: bfloat16 [8192, 2048], P('fs')
- up_grad_out: float32 [2048, 4096], P('fs', 'tp')
All inputs are finite; a program needn't handle non-finite values.
Results may differ from a plain program's by a relative error of at most 0.013.
Values may be sent and summed in bfloat16 or wider, within the bound.
No kernel may reach another device: no remote copies, remote signals or barrier semaphores. Data moves between devices by JAX's collectives and lax.ppermute only.
A program may use at most 64 MiB of HBM per device.

v0:
```python
import jax
import jax.numpy as jnp
from jax import lax
from jax.sharding import Mesh
from jax.sharding import PartitionSpec as P

FS = ("fs_0", "fs_1")


def gathered_by_axis(array, axes, dim):
    for axis in reversed(axes):
        array = lax.all_gather(array, axis, axis=dim, tiled=True)
    return array


def from_everyone(array, axis):
    size = lax.axis_size(axis)
    return lax.all_to_all(
        jnp.broadcast_to(array[None], (size, *array.shape)), axis, 0, 0, tiled=True
    )


def over_copies(array, axis):
    return from_everyone(array, axis).astype(jnp.float32).sum(axis=0)


def sum_in_order(tiles, axes, sequence):
    inside = tiles.shape[1:]
    tiles = tiles.reshape(*(lax.axis_size(a) for a in axes), *inside)
    tiles = jnp.moveaxis(tiles, sequence, range(len(axes))).reshape(-1, *inside)
    for k in sequence:
        tiles = lax.psum_scatter(tiles, axes[k], scatter_dimension=0, tiled=True)
    return tiles[0]


def in_blocks(array, dim, size):
    shape = array.shape
    tiles = array.reshape(*shape[:dim], size, shape[dim] // size, *shape[dim + 1 :])
    return jnp.moveaxis(tiles, dim, 0)


def sum_by_axis_2(array, axes, sequence, dim):
    size = lax.axis_size(axes)
    return sum_in_order(in_blocks(array, dim, size), axes, sequence)


def per_device(fwd_input, saved_input, out_cotangent, up_weight, down_weight, up_grad_sum):
    row_count = fwd_input.shape[0]
    stacked = jnp.concatenate([fwd_input, saved_input], axis=0)
    up_whole = gathered_by_axis(up_weight, FS, 0)
    down_whole = gathered_by_axis(down_weight, FS, 1)
    pre_both = jnp.dot(stacked, up_whole, preferred_element_type=jnp.float32)
    pre_fwd = pre_both[:row_count]
    pre_bwd = pre_both[row_count:]
    positive = jnp.maximum(pre_fwd, 0.0)
    hidden = (positive * positive).astype(jnp.bfloat16)
    out_part = jnp.dot(hidden, down_whole, preferred_element_type=jnp.float32)
    layer_out = (
        over_copies(out_part.astype(jnp.bfloat16), "tp").astype(jnp.float32).astype(jnp.bfloat16)
    )
    d_hidden = lax.dot_general(
        out_cotangent, down_whole, (((1,), (1,)), ((), ())), preferred_element_type=jnp.float32
    )
    d_pre = (d_hidden * 2.0 * jnp.maximum(pre_bwd, 0.0)).astype(jnp.bfloat16)
    in_part = lax.dot_general(
        d_pre, up_whole, (((1,), (1,)), ((), ())), preferred_element_type=jnp.float32
    )
    input_grad = (
        over_copies(in_part.astype(jnp.bfloat16), "tp").astype(jnp.float32).astype(jnp.bfloat16)
    )
    grad_part = sum_by_axis_2(
        lax.dot_general(
            saved_input, d_pre, (((0,), (0,)), ((), ())), preferred_element_type=jnp.float32
        ),
        FS,
        (1, 0),
        0,
    )
    grad_scale = float(row_count * lax.axis_size(FS)) ** (-0.5)
    return (layer_out, input_grad, up_grad_sum + grad_part * grad_scale)


def solution(mesh):
    torus = Mesh(mesh.devices.reshape(16, 4, mesh.shape["tp"]), ("fs_0", "fs_1", "tp"))
    in_specs = (P(FS, None), P(FS, None), P(FS, None), P(FS, "tp"), P("tp", FS), P(FS, "tp"))
    out_specs = (P(FS, None), P(FS, None), P(FS, "tp"))
    return jax.shard_map(
        per_device, mesh=torus, in_specs=in_specs, out_specs=out_specs, check_vma=False
    )
```

profile of v0, /device:TPU:4, one launch (start us, length us, event | category | flops | bytes accessed | tf_op | source)
XLA Modules:
  0.0 330.4 jit_solution(14912935366155968894)
XLA Ops:
  7.2 14.2 %all_gather.12 = bf16[128,512]{1,0:T(8,128)(2,1)} all-gather(bf16[32,512]{1,0:T(8,128)(2,1)} %param.9), channel_id=1, replica_groups=mesh['fs_0'=16,'fs_1'=4,'tp'=8] {'fs_1'}, dimensions={0}, use_global_device_ids=true | all-gather | bytes 163840 | tf_op jit(solution)/shard_map/all_gather | solution.py:12
  21.5 12.9 %all_gather.14 = bf16[512,128]{0,1:T(8,128)(2,1)} all-gather(bf16[512,32]{0,1:T(8,128)(2,1)} %param.10), channel_id=1, replica_groups=mesh['fs_0'=16,'fs_1'=4,'tp'=8] {'fs_1'}, dimensions={1}, use_global_device_ids=true | all-gather | bytes 163840 | tf_op jit(solution)/shard_map/all_gather | solution.py:12
  34.5 0.0 reduce-scatter.3.cloned.1.call-start
  34.5 62.8 %all-gather.3.cloned.1.call-done = bf16[2048,512]{1,0:T(8,128)(2,1)} async-done(((bf16[128,512]{1,0:T(8,128)(2,1)}), bf16[2048,512]{1,0:T(8,128)(2,1)}) %all-gather.3.cloned.1.call-update) | async-done | bytes 2097168 | tf_op jit(solution)/shard_map/all_gather | solution.py:12
  97.3 2.6 fusion.2
  100.0 69.0 %all-gather.5.cloned.1.call-done = bf16[512,2048]{0,1:T(8,128)(2,1)} async-done(((bf16[512,128]{0,1:T(8,128)(2,1)}), bf16[512,2048]{0,1:T(8,128)(2,1)}) %all-gather.5.cloned.1.call-update) | async-done | bytes 2097168 | tf_op jit(solution)/shard_map/all_gather | solution.py:12
  169.0 2.0 fusion.1
  171.0 2.7 convolution_bitcast_fusion
  173.7 5.4 %copy.13 = f32[2048,512]{1,0:T(8,128)} copy(f32[2048,512]{0,1:T(8,128)} %convolution_bitcast_fusion) | data formatting | bytes 8388608 | tf_op jit(solution)/shard_map/dot_general | solution.py:72
  179.1 4.9 %copy.14 = f32[4,16,32,512]{3,2,1,0:T(8,128)} copy(f32[4,16,32,512]{3,2,0,1:T(8,128)} %bitcast.17) | data formatting | bytes 8388608 | tf_op jit(solution)/shard_map/transpose | solution.py:30
  184.1 1.6 copy-done.2
  185.6 0.8 convolution_convert_fusion
  186.5 2.5 broadcast_in_dim.5
  189.0 5.1 %all-to-all-start.1 = ((bf16[8,128,2048]{2,1,0:T(8,128)(2,1)}), bf16[8,128,2048]{2,1,0:T(8,128)(2,1)}, u32[]{:S(2)}, u32[]{:S(2)}) async-start(bf16[8,128,2048]{2,1,0:T(8,128)(2,1)} %broadcast_in_dim.5), calls=%async_computation.1 | async-start | bytes 8388608 | tf_op jit(solution)/shard_map/all_to_all | solution.py:18
  194.1 1.8 convolution_convert_fusion.1
  195.9 44.8 %all-to-all-done.1 = bf16[8,128,2048]{2,1,0:T(8,128)(2,1)} async-done(((bf16[8,128,2048]{2,1,0:T(8,128)(2,1)}), bf16[8,128,2048]{2,1,0:T(8,128)(2,1)}, u32[]{:S(2)}, u32[]{:S(2)}) %all-to-all-start.1) | async-done | bytes 4194336 | tf_op jit(solution)/shard_map/all_to_all | solution.py:18
  240.7 2.5 broadcast_in_dim.4
  243.2 7.7 %all-to-all-start = ((bf16[8,128,2048]{2,1,0:T(8,128)(2,1)}), bf16[8,128,2048]{2,1,0:T(8,128)(2,1)}, u32[]{:S(2)}, u32[]{:S(2)}) async-start(bf16[8,128,2048]{2,1,0:T(8,128)(2,1)} %broadcast_in_dim.4), calls=%async_computation | async-start | bytes 8388608 | tf_op jit(solution)/shard_map/all_to_all | solution.py:18
  250.8 0.6 reduce-scatter.5.cloned.1.call-update
  251.4 3.8 %reduce_sum.25 = bf16[128,2048]{1,0:T(8,128)(2,1)} reduce(bf16[8,128,2048]{2,1,0:T(8,128)(2,1)} %all-to-all-done.1, bf16[]{:T(256)} %constant.3.clone.1), dimensions={0}, to_apply=%region_1.0 | reduce | flops 1835008 | bytes 4718594 | tf_op jit(solution)/shard_map/reduce_sum | solution.py:24
  255.2 42.2 %all-to-all-done = bf16[8,128,2048]{2,1,0:T(8,128)(2,1)} async-done(((bf16[8,128,2048]{2,1,0:T(8,128)(2,1)}), bf16[8,128,2048]{2,1,0:T(8,128)(2,1)}, u32[]{:S(2)}, u32[]{:S(2)}) %all-to-all-start) | async-done | bytes 4194336 | tf_op jit(solution)/shard_map/all_to_all | solution.py:18
  297.4 3.9 %reduce_sum.24 = bf16[128,2048]{1,0:T(8,128)(2,1)} reduce(bf16[8,128,2048]{2,1,0:T(8,128)(2,1)} %all-to-all-done, bf16[]{:T(256)} %constant.3.clone.1), dimensions={0}, to_apply=%region_0.0 | reduce | flops 1835008 | bytes 4718594 | tf_op jit(solution)/shard_map/reduce_sum | solution.py:24
  301.3 21.1 %reduce-scatter.5.cloned.1.call-done = f32[1,32,512]{2,1,0:T(8,128)} async-done(((f32[16,32,512]{2,1,0:T(8,128)}), f32[1,32,512]{2,1,0:T(8,128)}) %reduce-scatter.5.cloned.1.call-update) | async-done | bytes 65552 | tf_op jit(solution)/shard_map/reduce_scatter | solution.py:32
  322.4 1.5 bitcast_add_fusion
  (18 shorter events, 0.2 us)
Async XLA Ops:
  7.2 161.8 %copy-start = (bf16[128,2048]{1,0:T(8,128)(2,1)S(1)}, bf16[128,2048]{1,0:T(8,128)(2,1)}, u32[]{:S(2)}) copy-start(bf16[128,2048]{1,0:T(8,128)(2,1)} %param.8) | copy-start | bytes 1572868
  7.2 90.2 %all-gather.3.cloned.1.call-start = ((), (), s32[]{:S(2)}) async-start(), calls=%async_computation.4 | async-start | bytes 2228224 | tf_op jit(solution)/shard_map/all_gather | solution.py:12
  21.5 147.5 %all-gather.5.cloned.1.call-start = ((), (), s32[]{:S(2)}) async-start(), calls=%async_computation.5 | async-start | bytes 2228224 | tf_op jit(solution)/shard_map/all_gather | solution.py:12
  34.5 216.3 %reduce-scatter.3.cloned.1.call-start = ((), (), s32[]{:S(2)}) async-start(), calls=%async_computation.6 | async-start | bytes 5242880 | tf_op jit(solution)/shard_map/reduce_scatter | solution.py:32
  100.0 73.7 %copy-start.4 = (f32[256,512]{1,0:T(8,128)}, f32[256,512]{1,0:T(8,128)S(1)}, u32[]{:S(2)}) copy-start(f32[256,512]{1,0:T(8,128)S(1)} %fusion.2) | copy-start | bytes 1572868
  100.0 71.0 %copy-start.3 = (bf16[128,2048]{1,0:T(8,128)(2,1)S(1)}, bf16[128,2048]{1,0:T(8,128)(2,1)}, u32[]{:S(2)}) copy-start(bf16[128,2048]{1,0:T(8,128)(2,1)} %param.7) | copy-start | bytes 1572868
  184.1 1.6 copy-start.2
  189.0 5.2 %copy-start.1 = (bf16[512,2048]{0,1:T(8,128)(2,1)S(1)}, bf16[512,2048]{0,1:T(8,128)(2,1)}, u32[]{:S(2)}) copy-start(bf16[512,2048]{0,1:T(8,128)(2,1)} %all-gather.5.cloned.1.call-done) | copy-start | bytes 6291460
  189.0 51.7 %all-to-all-start.1 = ((bf16[8,128,2048]{2,1,0:T(8,128)(2,1)}), bf16[8,128,2048]{2,1,0:T(8,128)(2,1)}, u32[]{:S(2)}, u32[]{:S(2)}) async-start(bf16[8,128,2048]{2,1,0:T(8,128)(2,1)} %broadcast_in_dim.5), calls=%async_computation.1 | async-start | bytes 8388608 | tf_op jit(solution)/shard_map/all_to_all | solution.py:18
  243.2 54.2 %all-to-all-start = ((bf16[8,128,2048]{2,1,0:T(8,128)(2,1)}), bf16[8,128,2048]{2,1,0:T(8,128)(2,1)}, u32[]{:S(2)}, u32[]{:S(2)}) async-start(bf16[8,128,2048]{2,1,0:T(8,128)(2,1)} %broadcast_in_dim.4), calls=%async_computation | async-start | bytes 8388608 | tf_op jit(solution)/shard_map/all_to_all | solution.py:18
  250.8 71.5 %reduce-scatter.5.cloned.1.call-start = ((), (), s32[]{:S(2)}) async-start(), calls=%async_computation.7 | async-start | bytes 1114112 | tf_op jit(solution)/shard_map/reduce_scatter | solution.py:32
  255.2 67.1 %copy-start.5 = (f32[32,512]{1,0:T(8,128)S(1)}, f32[32,512]{1,0:T(8,128)}, u32[]{:S(2)}) copy-start(f32[32,512]{1,0:T(8,128)} %param.11) | copy-start | bytes 196612
Sparse Core Ops, SparseCore 0:
  21.6 75.7 all-gather.2
  99.4 69.5 all-gather.4
  184.2 51.4 reduce-scatter.2
  254.1 68.1 reduce-scatter.4
where the time goes:
time: 331 us; the launch traced here: 330 us
  waiting for transfers between devices  240 us (73%)
  blocking collectives  27.2 us (8%)
  local copies, waits for them, and re-layouts  16.9 us (5%)
  between operations  13.8 us (4%)
  starting transfers between devices  12.9 us (4%)
  matrix products  9.91 us (3%)
  other arithmetic  9.2 us (3%)
    all_gather x2, waiting for transfers between devices, gathered_by_axis(): array = lax.all_gather(array, axis, axis=dim, tiled=True)  132 us
    all_to_all x2, waiting for transfers between devices, from_everyone(): lax.all_to_all(jnp.broadcast_to(array[None], (size, *array.shape)), axis,...  87 us
    all_gather x2, blocking collectives, gathered_by_axis(): array = lax.all_gather(array, axis, axis=dim, tiled=True)  27.2 us
    reduce_scatter x2, waiting for transfers between devices, sum_in_order(): tiles = lax.psum_scatter(tiles, axes[k], scatter_dimension=0, tiled=True)  21.1 us
    all_to_all x2, starting transfers between devices, from_everyone(): lax.all_to_all(jnp.broadcast_to(array[None], (size, *array.shape)), axis,...  12.8 us
    reduce_sum x2, other arithmetic, over_copies(): return from_everyone(array, axis).astype(jnp.float32).sum(axis=0)  7.72 us
  transfers between devices with their start and end apart: 6, of which 5 were waited for; matrix products, arithmetic and copies ran while one was open for 5% of the time, Pallas kernels for 0%

commit v1 on v0

v1 whole, which is shorter than its diff:
```python
import jax
import jax.numpy as jnp
from jax import lax
from jax.sharding import PartitionSpec as P

NZ, NY = 16, 4
BOTH = ("fs", "tp")


def group_lists(n_tp):
    def device(z, y, t):
        return ((z % NZ) * NY + y % NY) * n_tp + t

    far = [
        [device(2 * i + a, 2 * j + b, t) for i in range(NZ // 2) for j in range(NY // 2)]
        for a in range(2)
        for b in range(2)
        for t in range(n_tp)
    ]
    near = []
    for t in range(n_tp):
        c = t % 2
        for r in range(NZ // 2):
            for q in range(NY // 2):
                members = [
                    (2 * r + c + dz, 2 * q + c + dy) for dz in range(2) for dy in range(2)
                ]
                members.sort(key=lambda m: (m[0] % 2, m[1] % 2))
                near.append([device(z, y, t) for z, y in members])
    return far, near


def exchange(array, groups):
    return lax.all_to_all(array, BOTH, 0, 0, axis_index_groups=groups, tiled=True)


def copies(array, n):
    return jnp.broadcast_to(array[None], (n, *array.shape))


def dot(a, b, dims):
    return lax.dot_general(a, b, (dims, ((), ())), preferred_element_type=jnp.float32)


def solution(mesh):
    n_tp = mesh.shape["tp"]
    n_fs = mesh.shape["fs"]
    far, near = group_lists(n_tp)
    n_far, n_near = len(far[0]), len(near[0])

    def per_device(fwd_input, saved_input, out_cotangent, up_weight, down_weight, up_grad_sum):
        rows, width = fwd_input.shape
        own, block = up_weight.shape
        bf16, f32 = jnp.bfloat16, jnp.float32
        w = jnp.concatenate([up_weight, down_weight.T], axis=0)
        w = exchange(copies(w, n_far), far)
        s = saved_input.reshape(rows, NZ // 2, 2, NY // 2, 2, own)
        s = s.transpose(2, 4, 0, 1, 3, 5).reshape(n_near, rows, n_far * own)
        w = w.reshape(n_far * 2 * own, block)
        packed = exchange(jnp.concatenate([copies(w, n_near), s], axis=1), near)
        w = packed[:, : n_far * 2 * own].reshape(2, 2, NZ // 2, NY // 2, 2, own, block)
        w = w.transpose(4, 2, 0, 3, 1, 5, 6).reshape(2, width, block)
        up, down_t = w[0], w[1]
        s = packed[:, n_far * 2 * own :].reshape(n_near * rows, n_far * own)

        pre_bwd = dot(saved_input, up, ((1,), (0,)))
        d_hidden = dot(out_cotangent, down_t, ((1,), (0,)))
        d_pre = (d_hidden * 2.0 * jnp.maximum(pre_bwd, 0.0)).astype(bf16)
        d_all = exchange(copies(d_pre, n_near), near).reshape(n_near * rows, block)

        pre_fwd = dot(fwd_input, up, ((1,), (0,)))
        positive = jnp.maximum(pre_fwd, 0.0)
        hidden = (positive * positive).astype(bf16)
        out_part = dot(hidden, down_t, ((1,), (1,))).astype(bf16)
        in_part = dot(d_pre, up, ((1,), (1,))).astype(bf16)

        grad = dot(s, d_all, ((0,), (0,))).astype(bf16).reshape(n_far, own, block)
        grad = exchange(grad, far).astype(f32).sum(axis=0)
        scale = float(rows * n_fs) ** (-0.5)
        up_grad_out = up_grad_sum + grad * scale

        piece = rows // n_tp
        parts = jnp.stack(
            [out_part.reshape(n_tp, piece, width), in_part.reshape(n_tp, piece, width)], axis=1
        )
        parts = lax.all_to_all(parts, "tp", 0, 0, tiled=True)
        sums = parts.astype(f32).sum(axis=0).astype(bf16)
        sums = lax.all_to_all(copies(sums, n_tp), "tp", 0, 0, tiled=True)
        layer_out = sums[:, 0].reshape(rows, width)
        input_grad = sums[:, 1].reshape(rows, width)
        return layer_out, input_grad, up_grad_out

    split = P("fs", None)
    in_specs = (split, split, split, P("fs", "tp"), P("tp", "fs"), P("fs", "tp"))
    return jax.shard_map(
        per_device,
        mesh=mesh,
        in_specs=in_specs,
        out_specs=(split, split, P("fs", "tp")),
        check_vma=False,
    )
```

time: 331 us -> 226 us (0.68)
  the two profiles are of different devices: /device:TPU:4 before, /device:TPU:8 now
where the time goes in v1:
time: 226 us; the launch traced here: 225 us
  waiting for transfers between devices  119 us (53%)
  starting transfers between devices  37.1 us (16%)
  blocking collectives  33.9 us (15%)
  local copies, waits for them, and re-layouts  20.9 us (9%)
  matrix products  9.64 us (4%)
  other arithmetic  3.39 us (2%)
    all_to_all x3, waiting for transfers between devices, exchange(): lax.all_to_all(array, BOTH, 0, 0, axis_index_groups=groups, tiled=True)  89.7 us
    all_to_all x1, blocking collectives, exchange(): lax.all_to_all(array, BOTH, 0, 0, axis_index_groups=groups, tiled=True)  33.9 us
    all_to_all x3, starting transfers between devices, exchange(): lax.all_to_all(array, BOTH, 0, 0, axis_index_groups=groups, tiled=True)  28.7 us
    all_to_all x1, waiting for transfers between devices, per_device(): parts = lax.all_to_all(parts, 'tp', 0, 0, tiled=True)  15.8 us
    all_to_all x1, waiting for transfers between devices, per_device(): sums = lax.all_to_all(copies(sums, n_tp), 'tp', 0, 0, tiled=True)  13.6 us
    dot_general x5, matrix products, dot(): lax.dot_general(a, b, (dims, ((), ())), preferred_element_type=jnp.float32)  9.64 us
    slice x2, local copies, waits for them, and re-layouts, per_device(): packed[:, :n_far * 2 * own].reshape(2, 2, NZ // 2, NY // 2, 2, own, block)  8.85 us
    all_to_all x1, starting transfers between devices, per_device(): parts = lax.all_to_all(parts, 'tp', 0, 0, tiled=True)  4.83 us
  transfers between devices with their start and end apart: 5, of which 5 were waited for; matrix products, arithmetic and copies ran while one was open for 2% of the time, Pallas kernels for 0%

profile of v1, /device:TPU:8, one launch (start us, length us, event | category | flops | bytes accessed | tf_op | source)
XLA Modules:
  0.0 224.8 jit_solution(15401743978389936908)
XLA Ops:
  0.7 0.9 pad_maximum_fusion.2
  1.5 1.1 broadcast_in_dim.10
  2.6 16.9 %all-to-all-start = ((bf16[16,64,512]{2,1,0:T(8,128)(2,1)}), bf16[16,64,512]{2,1,0:T(8,128)(2,1)S(1)}, u32[]{:S(2)}, u32[]{:S(2)}) async-start(bf16[16,64,512]{2,1,0:T(8,128)(2,1)} %broadcast_in_dim.10), calls=%async_computation | async-start | bytes 2097152 | tf_op jit(solution)/shard_map/all_to_all | solution.py:34
  19.9 51.1 %all-to-all-done = bf16[16,64,512]{2,1,0:T(8,128)(2,1)S(1)} async-done(((bf16[16,64,512]{2,1,0:T(8,128)(2,1)}), bf16[16,64,512]{2,1,0:T(8,128)(2,1)S(1)}, u32[]{:S(2)}, u32[]{:S(2)}) %all-to-all-start) | async-done | bytes 1048608 | tf_op jit(solution)/shard_map/all_to_all | solution.py:34
  72.7 33.9 %all_to_all.30 = bf16[4,1152,512]{1,2,0:T(8,128)(2,1)S(1)} all-to-all(bf16[4,1152,512]{1,2,0:T(8,128)(2,1)S(1)} %pad_maximum_fusion), channel_id=1, replica_groups={{0,8,32,40},{16,24,48,56},{64,72,96,104},{80,88,112,120},{128,136,160,1..., dimensions={0} | all-to-all | bytes 9437184 | tf_op jit(solution)/shard_map/all_to_all | solution.py:34
  106.7 2.1 copy-done.2
  108.8 2.6 %slice.26 = bf16[4,1024,512]{1,2,0:T(8,128)(2,1)} slice(bf16[4,1152,512]{1,2,0:T(8,128)(2,1)S(1)} %all_to_all.30), slice={[0:4], [0:1024], [0:512]} | slice | bytes 8388608 | tf_op jit(solution)/shard_map/slice | solution.py:61
  111.4 6.2 %copy.22 = bf16[4,1024,512]{2,1,0:T(8,128)(2,1)} copy(bf16[4,1024,512]{1,2,0:T(8,128)(2,1)} %slice.26) | data formatting | bytes 8388608 | tf_op jit(solution)/shard_map/slice | solution.py:61
  117.7 2.5 %fusion.8 = (bf16[1,8,2,2,2,32,512]{6,5,0,3,1,4,2:T(8,128)(2,1)S(1)}, bf16[1,8,2,2,2,32,512]{6,5,0,3,1,4,2:T(8,128)(2,1)S(1)}) fusion(bf16[2,8,2,2,2,32,512]{6,5,0,3,1,4,2:T(8,128)(2,1)} %bitcast.40), kind=kLoop, calls=%fused_computation.19 | loop fusion | bytes 8388608 | tf_op jit(solution)/shard_map/slice | solution.py:63
  120.5 1.4 copy-done.1
  122.6 4.0 %convolution_convert_fusion.1 = bf16[128,2048]{1,0:T(8,128)(2,1)S(1)} fusion(bf16[2048,512]{1,0:T(8,128)(2,1)} %bitcast.39, bf16[2048,512]{1,0:T(8,128)(2,1)S(1)} %bitcast.35, bf16[128,2048]{1,0:T(8,128)(2,1)S(1)} %copy-done), kind=kOutput, calls=%fused_computation.2 | convolution fusion | flops 537329664 | bytes 5242880 | tf_op jit(solution)/shard_map/dot_general | solution.py:42
  126.7 1.8 fusion.4
  129.3 1.1 pad_maximum_fusion.1
  130.4 4.8 %all-to-all-start.2 = ((bf16[8,2,16,2048]{3,2,1,0:T(8,128)(2,1)}), bf16[8,2,16,2048]{3,2,1,0:T(8,128)(2,1)S(1)}, u32[]{:S(2)}, u32[]{:S(2)}) async-start(bf16[8,2,16,2048]{3,2,1,0:T(8,128)(2,1)} %pad_maximum_fusion.1), calls=%async_computation.2 | async-start | bytes 2097152 | tf_op jit(solution)/shard_map/all_to_all | solution.py:86
  135.3 15.8 %all-to-all-done.2 = bf16[8,2,16,2048]{3,2,1,0:T(8,128)(2,1)S(1)} async-done(((bf16[8,2,16,2048]{3,2,1,0:T(8,128)(2,1)}), bf16[8,2,16,2048]{3,2,1,0:T(8,128)(2,1)S(1)}, u32[]{:S(2)}, u32[]{:S(2)}) %all-to-all-start.2) | async-done | bytes 1048608 | tf_op jit(solution)/shard_map/all_to_all | solution.py:86
  152.0 5.6 %all-to-all-start.4 = ((bf16[4,128,512]{2,1,0:T(8,128)(2,1)}), bf16[4,128,512]{2,1,0:T(8,128)(2,1)S(1)}, u32[]{:S(2)}, u32[]{:S(2)}) async-start(bf16[4,128,512]{2,1,0:T(8,128)(2,1)} %broadcast_in_dim.14), calls=%async_computation.4 | async-start | bytes 1048576 | tf_op jit(solution)/shard_map/all_to_all | solution.py:34
  157.8 5.9 %all-to-all-done.4 = bf16[4,128,512]{2,1,0:T(8,128)(2,1)S(1)} async-done(((bf16[4,128,512]{2,1,0:T(8,128)(2,1)}), bf16[4,128,512]{2,1,0:T(8,128)(2,1)S(1)}, u32[]{:S(2)}, u32[]{:S(2)}) %all-to-all-start.4) | async-done | bytes 524320 | tf_op jit(solution)/shard_map/all_to_all | solution.py:34
  163.7 1.1 broadcast_in_dim.13
  164.8 3.6 %all-to-all-start.3 = ((bf16[8,2,16,2048]{3,2,1,0:T(8,128)(2,1)}), bf16[8,2,16,2048]{3,2,1,0:T(8,128)(2,1)S(1)}, u32[]{:S(2)}, u32[]{:S(2)}) async-start(bf16[8,2,16,2048]{3,2,1,0:T(8,128)(2,1)} %broadcast_in_dim.13), calls=%async_computation.3 | async-start | bytes 2097152 | tf_op jit(solution)/shard_map/all_to_all | solution.py:88
  168.4 2.3 %fusion = bf16[512,512]{1,0:T(8,128)(2,1)} fusion(bf16[4,128,512]{2,1,0:T(8,128)(2,1)S(1)} %all-to-all-done.4, bf16[4,1152,512]{1,2,0:T(8,128)(2,1)} %copy-done.2), kind=kOutput, calls=%fused_computation.4 | convolution fusion | flops 268697600 | bytes 1572864 | tf_op jit(solution)/shard_map/dot_general | solution.py:42
  170.7 13.6 %all-to-all-done.3 = bf16[8,2,16,2048]{3,2,1,0:T(8,128)(2,1)S(1)} async-done(((bf16[8,2,16,2048]{3,2,1,0:T(8,128)(2,1)}), bf16[8,2,16,2048]{3,2,1,0:T(8,128)(2,1)S(1)}, u32[]{:S(2)}, u32[]{:S(2)}) %all-to-all-start.3) | async-done | bytes 1048608 | tf_op jit(solution)/shard_map/all_to_all | solution.py:88
  184.2 6.1 %all-to-all-start.5 = ((bf16[16,32,512]{2,1,0:T(8,128)(2,1)}), bf16[16,32,512]{2,1,0:T(8,128)(2,1)S(1)}, u32[]{:S(2)}, u32[]{:S(2)}) async-start(bf16[16,32,512]{2,1,0:T(8,128)(2,1)} %bitcast.18), calls=%async_computation.5 | async-start | bytes 1048576 | tf_op jit(solution)/shard_map/all_to_all | solution.py:34
  190.4 1.0 fusion.9
  191.4 32.7 %all-to-all-done.5 = bf16[16,32,512]{2,1,0:T(8,128)(2,1)S(1)} async-done(((bf16[16,32,512]{2,1,0:T(8,128)(2,1)}), bf16[16,32,512]{2,1,0:T(8,128)(2,1)S(1)}, u32[]{:S(2)}, u32[]{:S(2)}) %all-to-all-start.5) | async-done | bytes 524320 | tf_op jit(solution)/shard_map/all_to_all | solution.py:34
  (24 shorter events, 5.7 us)
Async XLA Ops:
  0.6 122.0 %copy-start = (bf16[128,2048]{1,0:T(8,128)(2,1)S(1)}, bf16[128,2048]{1,0:T(8,128)(2,1)}, u32[]{:S(2)}) copy-start(bf16[128,2048]{1,0:T(8,128)(2,1)} %param.6) | copy-start | bytes 1572868
  0.6 18.9 %copy-start.3 = (bf16[128,2048]{1,0:T(8,128)(2,1)S(1)}, bf16[128,2048]{1,0:T(8,128)(2,1)}, u32[]{:S(2)}) copy-start(bf16[128,2048]{1,0:T(8,128)(2,1)} %param.7) | copy-start | bytes 1572868
  2.6 68.4 %all-to-all-start = ((bf16[16,64,512]{2,1,0:T(8,128)(2,1)}), bf16[16,64,512]{2,1,0:T(8,128)(2,1)S(1)}, u32[]{:S(2)}, u32[]{:S(2)}) async-start(bf16[16,64,512]{2,1,0:T(8,128)(2,1)} %broadcast_in_dim.10), calls=%async_computation | async-start | bytes 2097152 | tf_op jit(solution)/shard_map/all_to_all | solution.py:34
  106.7 2.1 copy-start.2
  120.3 1.5 copy-start.4
  120.5 1.4 copy-start.1
  130.4 20.8 %all-to-all-start.2 = ((bf16[8,2,16,2048]{3,2,1,0:T(8,128)(2,1)}), bf16[8,2,16,2048]{3,2,1,0:T(8,128)(2,1)S(1)}, u32[]{:S(2)}, u32[]{:S(2)}) async-start(bf16[8,2,16,2048]{3,2,1,0:T(8,128)(2,1)} %pad_maximum_fusion.1), calls=%async_computation.2 | async-start | bytes 2097152 | tf_op jit(solution)/shard_map/all_to_all | solution.py:86
  152.0 11.7 %all-to-all-start.4 = ((bf16[4,128,512]{2,1,0:T(8,128)(2,1)}), bf16[4,128,512]{2,1,0:T(8,128)(2,1)S(1)}, u32[]{:S(2)}, u32[]{:S(2)}) async-start(bf16[4,128,512]{2,1,0:T(8,128)(2,1)} %broadcast_in_dim.14), calls=%async_computation.4 | async-start | bytes 1048576 | tf_op jit(solution)/shard_map/all_to_all | solution.py:34
  164.8 19.4 %all-to-all-start.3 = ((bf16[8,2,16,2048]{3,2,1,0:T(8,128)(2,1)}), bf16[8,2,16,2048]{3,2,1,0:T(8,128)(2,1)S(1)}, u32[]{:S(2)}, u32[]{:S(2)}) async-start(bf16[8,2,16,2048]{3,2,1,0:T(8,128)(2,1)} %broadcast_in_dim.13), calls=%async_computation.3 | async-start | bytes 2097152 | tf_op jit(solution)/shard_map/all_to_all | solution.py:88
  170.7 53.5 %copy-start.5 = (f32[32,512]{1,0:T(8,128)S(1)}, f32[32,512]{1,0:T(8,128)}, u32[]{:S(2)}) copy-start(f32[32,512]{1,0:T(8,128)} %param.11) | copy-start | bytes 196612
  184.2 39.8 %all-to-all-start.5 = ((bf16[16,32,512]{2,1,0:T(8,128)(2,1)}), bf16[16,32,512]{2,1,0:T(8,128)(2,1)S(1)}, u32[]{:S(2)}, u32[]{:S(2)}) async-start(bf16[16,32,512]{2,1,0:T(8,128)(2,1)} %bitcast.18), calls=%async_computation.5 | async-start | bytes 1048576 | tf_op jit(solution)/shard_map/all_to_all | solution.py:34
